TPU v7x, 32 devices: a whole 2x2x4 slice. The times are simulated.
32 devices in a mesh: fs: 8 (over z, y), tp: 4 (over x, core).
Axes of the slice: x: 2, y: 2, z: 4, core: 2. Of those that a mesh axis runs over, the one named last changes fastest.
Arguments:
- saved_inputs: bfloat16 [16384, 4096], P('fs'), may hold values from -6 to 6
- value_cot: bfloat16 [16384, 1024], P('fs', 'tp'), may hold values from -6 to 6
- gate_cot: bfloat16 [16384, 1024], P('fs', 'tp'), may hold values from -6 to 6
- point_inputs: bfloat16 [16384, 1024], P('fs'), may hold values from -6 to 6
- point_cot: bfloat16 [16384, 1024], P('fs', 'tp'), may hold values from -6 to 6
- master_value: float32 [4096, 1024], P('fs', 'tp'), may hold values from -6 to 6
- master_gate: float32 [4096, 1024], P('fs', 'tp'), may hold values from -6 to 6
- master_point: float32 [1024, 1024], P('fs', 'tp'), may hold values from -6 to 6
- factor_value: bfloat16 [4096, 256], P('fs'), may hold values from -160 to 160
- factor_gate: bfloat16 [4096, 256], P('fs'), may hold values from -160 to 160
- factor_point: bfloat16 [1024, 256], P('fs'), may hold values from -160 to 160
- first_value: float32 [256, 1024], P('fs', 'tp'), may hold values from -6 to 6
- first_gate: float32 [256, 1024], P('fs', 'tp'), may hold values from -6 to 6
- first_point: float32 [256, 1024], P('fs', 'tp'), may hold values from -6 to 6
- second_value: float32 [256, 1024], P('fs', 'tp'), may hold values from 0.2 to 2
- second_gate: float32 [256, 1024], P('fs', 'tp'), may hold values from 0.2 to 2
- second_point: float32 [256, 1024], P('fs', 'tp'), may hold values from 0.2 to 2
Outputs:
- new_value: float32 [4096, 1024], P('fs', 'tp')
- new_gate: float32 [4096, 1024], P('fs', 'tp')
- new_point: float32 [1024, 1024], P('fs', 'tp')
- copy_value: bfloat16 [4096, 1024], P(None, 'tp')
- copy_gate: bfloat16 [4096, 1024], P(None, 'tp')
- copy_point: bfloat16 [1024, 1024], P(None, 'tp')
- next_first_value: float32 [256, 1024], P('fs', 'tp')
- next_first_gate: float32 [256, 1024], P('fs', 'tp')
- next_first_point: float32 [256, 1024], P('fs', 'tp')
- next_second_value: float32 [256, 1024], P('fs', 'tp')
- next_second_gate: float32 [256, 1024], P('fs', 'tp')
- next_second_point: float32 [256, 1024], P('fs', 'tp')
All inputs are finite; a program needn't handle non-finite values.
Results may differ from a plain program's by a relative error of at most 0.0055.
Values may be sent and summed in bfloat16 or wider, within the bound.
A program may use at most 128 MiB of HBM per device.

v0:
```python
import jax
import jax.numpy as jnp
from jax import lax
from jax.sharding import PartitionSpec as P


def contract_rows(left, right):
    return lax.dot_general(
        left, right, (((0,), (0,)), ((), ())), preferred_element_type=jnp.float32
    )


def contract_split(projected, cot):
    upper = projected.astype(jnp.bfloat16)
    lower = (projected - upper.astype(jnp.float32)).astype(jnp.bfloat16)
    return contract_rows(upper, cot) + contract_rows(lower, cot)


def moments(low, first_old, second_old):
    first = 0.8 * first_old + 0.2 * low
    second = 0.9 * second_old + 0.1 * low * low
    return (first, second, first / (jnp.sqrt(second) + 1e-08))


def local(
    saved_inputs,
    value_cot,
    gate_cot,
    point_inputs,
    point_cot,
    master_value,
    master_gate,
    master_point,
    factor_value,
    factor_gate,
    factor_point,
    first_value,
    first_gate,
    first_point,
    second_value,
    second_gate,
    second_point,
):
    total = saved_inputs.shape[0] * lax.axis_size("fs")
    columns = saved_inputs
    proj_value = jnp.dot(
        columns,
        lax.all_gather(factor_value, "fs", axis=0, tiled=True),
        preferred_element_type=jnp.float32,
    )
    proj_gate = jnp.dot(
        columns,
        lax.all_gather(factor_gate, "fs", axis=0, tiled=True),
        preferred_element_type=jnp.float32,
    )
    columns = point_inputs
    proj_point = jnp.dot(
        columns,
        lax.all_gather(factor_point, "fs", axis=0, tiled=True),
        preferred_element_type=jnp.float32,
    )
    low_value = contract_split(proj_value, value_cot)
    low_gate = contract_split(proj_gate, gate_cot)
    low_point = contract_split(proj_point, point_cot)
    summed = (
        lax.psum_scatter(low_value, "fs", scatter_dimension=0, tiled=True),
        lax.psum_scatter(low_gate, "fs", scatter_dimension=0, tiled=True),
        lax.psum_scatter(low_point, "fs", scatter_dimension=0, tiled=True),
    )
    fv, sv, dv = moments(summed[0] / total, first_value, second_value)
    fg, sg, dg = moments(summed[1] / total, first_gate, second_gate)
    fpt, spt, dpt = moments(summed[2] / total, first_point, second_point)
    whole_v, whole_g, whole_p = (
        lax.all_gather(dv, "fs", axis=0, tiled=True),
        lax.all_gather(dg, "fs", axis=0, tiled=True),
        lax.all_gather(dpt, "fs", axis=0, tiled=True),
    )
    full_v = jnp.dot(factor_value.astype(jnp.float32), whole_v, precision=lax.Precision.HIGHEST)
    full_g = jnp.dot(factor_gate.astype(jnp.float32), whole_g, precision=lax.Precision.HIGHEST)
    full_p = jnp.dot(factor_point.astype(jnp.float32), whole_p, precision=lax.Precision.HIGHEST)
    squares = lax.psum(
        (jnp.sum(full_v * full_v), jnp.sum(full_g * full_g), jnp.sum(full_p * full_p)), ("fs", "tp")
    )
    spread = lax.axis_size("fs") * lax.axis_size("tp")
    entries_in = full_v.shape[0] * full_v.shape[1] * spread
    entries_point = full_p.shape[0] * full_p.shape[1] * spread
    new_v = master_value - 0.1 * lax.rsqrt(squares[0] / entries_in + 1e-06) * full_v
    new_g = master_gate - 0.1 * lax.rsqrt(squares[1] / entries_in + 1e-06) * full_g
    new_p = master_point - 0.1 * lax.rsqrt(squares[2] / entries_point + 1e-06) * full_p
    copy_v, copy_g, copy_p = (
        lax.all_gather(new_v.astype(jnp.bfloat16), "fs", axis=0, tiled=True),
        lax.all_gather(new_g.astype(jnp.bfloat16), "fs", axis=0, tiled=True),
        lax.all_gather(new_p.astype(jnp.bfloat16), "fs", axis=0, tiled=True),
    )
    return (new_v, new_g, new_p, copy_v, copy_g, copy_p, fv, fg, fpt, sv, sg, spt)


def solution(mesh):
    return jax.shard_map(
        local,
        mesh=mesh,
        in_specs=(
            P("fs", None),
            P("fs", "tp"),
            P("fs", "tp"),
            P("fs", None),
            P("fs", "tp"),
            P("fs", "tp"),
            P("fs", "tp"),
            P("fs", "tp"),
            P("fs", None),
            P("fs", None),
            P("fs", None),
            P("fs", "tp"),
            P("fs", "tp"),
            P("fs", "tp"),
            P("fs", "tp"),
            P("fs", "tp"),
            P("fs", "tp"),
        ),
        out_specs=(
            P("fs", "tp"),
            P("fs", "tp"),
            P("fs", "tp"),
            P(None, "tp"),
            P(None, "tp"),
            P(None, "tp"),
            P("fs", "tp"),
            P("fs", "tp"),
            P("fs", "tp"),
            P("fs", "tp"),
            P("fs", "tp"),
            P("fs", "tp"),
        ),
        check_vma=False,
    )
```

profile of v0, /device:TPU:0, one launch (start us, length us, event | category | flops | bytes accessed | tf_op | source)
XLA Modules:
  0.0 531.6 jit_solution(17776841322710641022)
XLA Ops:
  7.2 0.0 copy-start
  7.2 0.0 reduce-scatter.8.cloned.1.call-start
  7.2 33.4 %all_gather.31 = bf16[1024,256]{1,0:T(8,128)(2,1)S(1)} all-gather(bf16[128,256]{1,0:T(8,128)(2,1)} %param.27), channel_id=1, replica_groups=mesh['fs'=8,'tp'=4] {'fs'}, dimensions={0}, use_global_device_ids=true | all-gather | bytes 589824 | tf_op jit(solution)/shard_map/all_gather | solution.py:59
  40.6 3.5 fusion.14
  44.1 0.5 fusion.1
  44.6 0.0 copy-start.5
  44.6 0.0 copy-start.8
  44.6 0.0 copy-start.9
  44.6 1.2 convolution_add_fusion
  45.8 0.0 reduce-scatter.8.cloned.1.call-update
  45.8 0.0 all-gather.7.cloned.1.call-start
  45.9 0.7 all-gather.7.cloned.1.call-update
  46.6 0.0 all-gather.5.cloned.1.call-start
  46.6 0.7 all-gather.5.cloned.1.call-update
  47.3 0.0 reduce-scatter.6.cloned.1.call-start
  47.4 0.2 copy.29
  47.6 61.6 %reduce-scatter.8.cloned.1.call-done = f32[32,256]{1,0:T(8,128)} async-done(((f32[256,256]{1,0:T(8,128)}), f32[32,256]{1,0:T(8,128)}) %reduce-scatter.8.cloned.1.call-update) | async-done | bytes 32784 | tf_op jit(solution)/shard_map/reduce_scatter | solution.py:68
  109.2 1.4 add_divide_fusion
  110.6 31.4 %all_gather.32 = f32[256,256]{1,0:T(8,128)S(1)} all-gather(f32[32,256]{1,0:T(8,128)S(1)} %get-tuple-element.33), channel_id=1, replica_groups=mesh['fs'=8,'tp'=4] {'fs'}, dimensions={0}, use_global_device_ids=true | all-gather | bytes 294912 | tf_op jit(solution)/shard_map/all_gather | solution.py:76
  142.0 18.3 %all-gather.7.cloned.1.call-done = bf16[4096,256]{1,0:T(8,128)(2,1)} async-done(((bf16[512,256]{1,0:T(8,128)(2,1)}), bf16[4096,256]{1,0:T(8,128)(2,1)}) %all-gather.7.cloned.1.call-update) | async-done | bytes 2097168 | tf_op jit(solution)/shard_map/all_gather | solution.py:53
  160.3 8.7 %fusion.13 = f32[2048,256]{1,0:T(8,128)S(1)} fusion(bf16[2048,4096]{1,0:T(8,128)(2,1)} %param.17, bf16[4096,256]{1,0:T(8,128)(2,1)} %all-gather.7.cloned.1.call-done), kind=kOutput, calls=%fused_computation.34 | convolution fusion | flops 4294967296 | bytes 20971520 | tf_op jit(solution)/shard_map/dot_general | solution.py:51
  169.0 0.5 fusion.4
  169.5 1.2 convolution_add_fusion.1
  170.7 0.0 reduce-scatter.6.cloned.1.call-update
  170.7 0.0 copy-start.2
  170.7 0.0 reduce-scatter.4.cloned.1.call-start
  170.8 39.5 %all-gather.5.cloned.1.call-done = bf16[4096,256]{1,0:T(8,128)(2,1)} async-done(((bf16[512,256]{1,0:T(8,128)(2,1)}), bf16[4096,256]{1,0:T(8,128)(2,1)}) %all-gather.5.cloned.1.call-update) | async-done | bytes 2097168 | tf_op jit(solution)/shard_map/all_gather | solution.py:48
  210.3 8.7 %fusion.12 = f32[2048,256]{1,0:T(8,128)S(1)} fusion(bf16[2048,4096]{1,0:T(8,128)(2,1)} %param.17, bf16[4096,256]{1,0:T(8,128)(2,1)} %all-gather.5.cloned.1.call-done), kind=kOutput, calls=%fused_computation.33 | convolution fusion | flops 4294967296 | bytes 20971520 | tf_op jit(solution)/shard_map/dot_general | solution.py:46
  219.0 0.5 fusion.7
  219.5 0.0 copy-start.6
  219.5 0.0 copy-start.10
  219.5 0.0 copy-start.11
  219.5 0.0 copy-start.12
  219.5 0.0 copy-start.13
  219.6 0.0 copy-start.3
  219.6 1.2 convolution_add_fusion.2
  220.8 0.0 reduce-scatter.4.cloned.1.call-update
  220.8 0.0 all-gather.9.cloned.1.call-start
  220.9 1.0 multiply_reduce_fusion.2
  221.8 52.9 %reduce-scatter.6.cloned.1.call-done = f32[32,256]{1,0:T(8,128)} async-done(((f32[256,256]{1,0:T(8,128)}), f32[32,256]{1,0:T(8,128)}) %reduce-scatter.6.cloned.1.call-update) | async-done | bytes 32784 | tf_op jit(solution)/shard_map/reduce_scatter | solution.py:67
  274.7 1.4 add_divide_fusion.1
  276.1 30.9 %all_gather.30 = f32[256,256]{1,0:T(8,128)S(1)} all-gather(f32[32,256]{1,0:T(8,128)S(1)} %get-tuple-element.36), channel_id=1, replica_groups=mesh['fs'=8,'tp'=4] {'fs'}, dimensions={0}, use_global_device_ids=true | all-gather | bytes 294912 | tf_op jit(solution)/shard_map/all_gather | solution.py:75
  307.1 32.6 %reduce-scatter.4.cloned.1.call-done = f32[32,256]{1,0:T(8,128)} async-done(((f32[256,256]{1,0:T(8,128)}), f32[32,256]{1,0:T(8,128)}) %reduce-scatter.4.cloned.1.call-update) | async-done | bytes 32784 | tf_op jit(solution)/shard_map/reduce_scatter | solution.py:66
  339.6 1.4 add_divide_fusion.2
  341.0 30.8 %all_gather.28 = f32[256,256]{1,0:T(8,128)S(1)} all-gather(f32[32,256]{1,0:T(8,128)S(1)} %get-tuple-element.39), channel_id=1, replica_groups=mesh['fs'=8,'tp'=4] {'fs'}, dimensions={0}, use_global_device_ids=true | all-gather | bytes 294912 | tf_op jit(solution)/shard_map/all_gather | solution.py:74
  371.9 1.2 multiply_reduce_fusion.1
  373.1 1.2 multiply_reduce_fusion
  374.3 38.0 %all-reduce = (f32[]{:T(128)}, f32[]{:T(128)}, f32[]{:T(128)}) all-reduce(f32[]{:T(128)} %get-tuple-element.42, f32[]{:T(128)} %get-tuple-element.44, f32[]{:T(128)} %get-tuple-element.46), channel_id=1, replica_groups=mesh['fs'=8,'tp'=4] {'fs','tp'}, use_global_device_ids=true, to_apply=%region_2.0 | all-reduce | flops 3 | bytes 24 | tf_op jit(solution)/shard_map/psum | solution.py:81
  412.9 0.8 fusion.11
  413.7 0.0 all-gather.9.cloned.1.call-update
  413.8 0.0 all-gather.11.cloned.1.call-start
  413.8 1.2 copy.30
  415.7 0.8 fusion.10
  416.6 0.0 all-gather.11.cloned.1.call-update
  416.6 0.1 copy.31
  417.4 0.8 copy.34
  418.2 29.7 %all_gather.35 = bf16[1024,256]{0,1:T(8,128)(2,1)S(1)} all-gather(bf16[128,256]{0,1:T(8,128)(2,1)S(1)} %get-tuple-element.27), channel_id=1, replica_groups=mesh['fs'=8,'tp'=4] {'fs'}, dimensions={0}, use_global_device_ids=true | all-gather | bytes 589824 | tf_op jit(solution)/shard_map/all_gather | solution.py:93
  447.9 1.0 copy.37
  448.9 1.0 copy.32
  449.9 1.0 copy.33
  450.9 19.2 %all-gather.9.cloned.1.call-done = bf16[4096,256]{0,1:T(8,128)(2,1)} async-done(((bf16[512,256]{0,1:T(8,128)(2,1)}), bf16[4096,256]{0,1:T(8,128)(2,1)}) %all-gather.9.cloned.1.call-update) | async-done | bytes 2097168 | tf_op jit(solution)/shard_map/all_gather | solution.py:91
  470.1 4.1 copy.35
  474.2 46.5 %all-gather.11.cloned.1.call-done = bf16[4096,256]{0,1:T(8,128)(2,1)} async-done(((bf16[512,256]{0,1:T(8,128)(2,1)}), bf16[4096,256]{0,1:T(8,128)(2,1)}) %all-gather.11.cloned.1.call-update) | async-done | bytes 2097168 | tf_op jit(solution)/shard_map/all_gather | solution.py:92
  520.7 4.1 copy.36
  (18 shorter events, 0.1 us)
Async XLA Ops:
  7.2 36.9 %copy-start = (bf16[2048,256]{1,0:T(8,128)(2,1)S(1)}, bf16[2048,256]{1,0:T(8,128)(2,1)}, u32[]{:S(2)}) copy-start(bf16[2048,256]{1,0:T(8,128)(2,1)} %param.21) | copy-start | bytes 3145732
  7.2 102.0 %reduce-scatter.8.cloned.1.call-start = ((), (), s32[]{:S(2)}) async-start(), calls=%async_computation.7 | async-start | bytes 294912 | tf_op jit(solution)/shard_map/reduce_scatter | solution.py:68
  44.6 2.8 copy-start.5
  44.6 64.6 %copy-start.8 = (f32[32,256]{1,0:T(8,128)S(1)}, f32[32,256]{1,0:T(8,128)}, u32[]{:S(2)}) copy-start(f32[32,256]{1,0:T(8,128)} %param.33) | copy-start | bytes 98308
  44.6 64.6 %copy-start.9 = (f32[32,256]{1,0:T(8,128)S(1)}, f32[32,256]{1,0:T(8,128)}, u32[]{:S(2)}) copy-start(f32[32,256]{1,0:T(8,128)} %param.30) | copy-start | bytes 98308
  45.8 114.4 %all-gather.7.cloned.1.call-start = ((), (), s32[]{:S(2)}) async-start(), calls=%async_computation.5 | async-start | bytes 2359296 | tf_op jit(solution)/shard_map/all_gather | solution.py:53
  46.6 163.7 %all-gather.5.cloned.1.call-start = ((), (), s32[]{:S(2)}) async-start(), calls=%async_computation.3 | async-start | bytes 2359296 | tf_op jit(solution)/shard_map/all_gather | solution.py:48
  47.3 227.4 %reduce-scatter.6.cloned.1.call-start = ((), (), s32[]{:S(2)}) async-start(), calls=%async_computation.6 | async-start | bytes 294912 | tf_op jit(solution)/shard_map/reduce_scatter | solution.py:67
  142.0 27.0 %copy-start.1 = (bf16[2048,256]{1,0:T(8,128)(2,1)S(1)}, bf16[2048,256]{1,0:T(8,128)(2,1)}, u32[]{:S(2)}) copy-start(bf16[2048,256]{1,0:T(8,128)(2,1)} %param.19) | copy-start | bytes 3145732
  170.7 48.2 %copy-start.2 = (bf16[2048,256]{1,0:T(8,128)(2,1)S(1)}, bf16[2048,256]{1,0:T(8,128)(2,1)}, u32[]{:S(2)}) copy-start(bf16[2048,256]{1,0:T(8,128)(2,1)} %param.18) | copy-start | bytes 3145732
  170.7 168.9 %reduce-scatter.4.cloned.1.call-start = ((), (), s32[]{:S(2)}) async-start(), calls=%async_computation.4 | async-start | bytes 294912 | tf_op jit(solution)/shard_map/reduce_scatter | solution.py:66
  219.5 1.4 copy-start.6
  219.5 55.2 %copy-start.10 = (f32[32,256]{1,0:T(8,128)S(1)}, f32[32,256]{1,0:T(8,128)}, u32[]{:S(2)}) copy-start(f32[32,256]{1,0:T(8,128)} %param.32) | copy-start | bytes 98308
  219.5 55.2 %copy-start.11 = (f32[32,256]{1,0:T(8,128)S(1)}, f32[32,256]{1,0:T(8,128)}, u32[]{:S(2)}) copy-start(f32[32,256]{1,0:T(8,128)} %param.29) | copy-start | bytes 98308
  219.5 120.1 %copy-start.12 = (f32[32,256]{1,0:T(8,128)S(1)}, f32[32,256]{1,0:T(8,128)}, u32[]{:S(2)}) copy-start(f32[32,256]{1,0:T(8,128)} %param.31) | copy-start | bytes 98308
  219.5 120.1 %copy-start.13 = (f32[32,256]{1,0:T(8,128)S(1)}, f32[32,256]{1,0:T(8,128)}, u32[]{:S(2)}) copy-start(f32[32,256]{1,0:T(8,128)} %param.28) | copy-start | bytes 98308
  219.6 152.3 %copy-start.3 = (bf16[512,256]{1,0:T(8,128)(2,1)S(1)}, bf16[512,256]{1,0:T(8,128)(2,1)}, u32[]{:S(2)}) copy-start(bf16[512,256]{1,0:T(8,128)(2,1)} %param.25) | copy-start | bytes 786436
  220.8 152.3 %copy-start.4 = (bf16[512,256]{1,0:T(8,128)(2,1)S(1)}, bf16[512,256]{1,0:T(8,128)(2,1)}, u32[]{:S(2)}) copy-start(bf16[512,256]{1,0:T(8,128)(2,1)} %param.26) | copy-start | bytes 786436
  220.8 249.3 %all-gather.9.cloned.1.call-start = ((), (), s32[]{:S(2)}) async-start(), calls=%async_computation.8 | async-start | bytes 2359296 | tf_op jit(solution)/shard_map/all_gather | solution.py:91
  413.7 2.9 copy-start.7
  413.8 106.9 %all-gather.11.cloned.1.call-start = ((), (), s32[]{:S(2)}) async-start(), calls=%async_computation.9 | async-start | bytes 2359296 | tf_op jit(solution)/shard_map/all_gather | solution.py:92
Sparse Core Ops, SparseCore 0:
  46.0 63.1 reduce-scatter.7
  111.3 48.9 all-gather.6
  162.4 47.8 all-gather.4
  214.0 60.6 reduce-scatter.5
  278.5 61.1 reduce-scatter.3
  413.9 56.1 all-gather.8
  472.1 48.5 all-gather.10
where the time goes:
time: 532 us
  waiting for transfers between devices  272 us (51%)
  blocking collectives  194 us (36%)
  matrix products  29.3 us (6%)
  between operations  16.4 us (3%)
  local copies, waits for them, and re-layouts  13.5 us (3%)
  other arithmetic  5.86 us (1%)
    reduce_scatter x1, waiting for transfers between devices, local(): lax.psum_scatter(low_point, 'fs', scatter_dimension=0, tiled=True)  61.6 us
    reduce_scatter x1, waiting for transfers between devices, local(): lax.psum_scatter(low_gate, 'fs', scatter_dimension=0, tiled=True)  52.9 us
    all_gather x1, waiting for transfers between devices, local(): lax.all_gather(new_g.astype(jnp.bfloat16), 'fs', axis=0, tiled=True)  46.5 us
    all_gather x1, waiting for transfers between devices, local(): lax.all_gather(factor_value, 'fs', axis=0, tiled=True)  39.5 us
    psum x1, blocking collectives, local(): lax.psum((jnp.sum(full_v * full_v), jnp.sum(full_g * full_g), jnp.sum(ful...  38 us
    all_gather x1, blocking collectives, local(): lax.all_gather(factor_point, 'fs', axis=0, tiled=True)  33.4 us
    reduce_scatter x1, waiting for transfers between devices, local(): lax.psum_scatter(low_value, 'fs', scatter_dimension=0, tiled=True)  32.6 us
    all_gather x1, blocking collectives, local(): lax.all_gather(dpt, 'fs', axis=0, tiled=True)  31.4 us
  transfers between devices with their start and end apart: 7, of which 7 were waited for; matrix products, arithmetic and copies ran while one was open for 7% of the time, Pallas kernels for 0%

commit v1 on v0

--- a/solution.py
+++ b/solution.py
@@ -41,6 +41,20 @@
     second_gate,
     second_point,
 ):
+
+    def _resolve_local_data(my_data, group_axis):
+        response, mat_out = (lax.axis_size(group_axis), lax.axis_index(group_axis))
+        front, work_now = (my_data, 1)
+        while work_now < response:
+            finding = lax.ppermute(
+                front, group_axis, list(map(lambda idx: (idx, idx ^ work_now), range(response)))
+            )
+            local_part = jnp.concatenate([front, finding], 0)
+            v_next = jnp.concatenate([finding, front], 0)
+            front = jnp.where(mat_out & work_now == 0, local_part, v_next)
+            work_now = 2 * work_now
+        return front
+
     total = saved_inputs.shape[0] * lax.axis_size("fs")
     columns = saved_inputs
     proj_value = jnp.dot(
@@ -73,7 +87,7 @@
     whole_v, whole_g, whole_p = (
         lax.all_gather(dv, "fs", axis=0, tiled=True),
         lax.all_gather(dg, "fs", axis=0, tiled=True),
-        lax.all_gather(dpt, "fs", axis=0, tiled=True),
+        _resolve_local_data(dpt, "fs"),
     )
     full_v = jnp.dot(factor_value.astype(jnp.float32), whole_v, precision=lax.Precision.HIGHEST)
     full_g = jnp.dot(factor_gate.astype(jnp.float32), whole_g, precision=lax.Precision.HIGHEST)

time: 532 us -> 533 us (level)
  blocking collectives: 194 us -> 163 us
  waiting for transfers between devices: 272 us -> 300 us
    all_gather x1 -> x0, blocking collectives: 31.4 us -> none  [local(): lax.all_gather(dpt, 'fs', axis=0, tiled=True)]
    all_gather x1, waiting for transfers between devices: 18.3 us -> 40 us  [local(): lax.all_gather(factor_gate, 'fs', axis=0, tiled=True)]
    ppermute x0 -> x3, waiting for transfers between devices: none -> 6.57 us  [_resolve_local_data(): lax.ppermute(front, group_axis, list(map(lambda idx: (idx, idx ^ work_now...]
    unnamed x37 -> x33, local copies, waits for them, and re-layouts: 13.5 us -> 13.5 us
  transfers between devices with their start and end apart: 7 -> 10, of which waited for: 7 -> 9; matrix products, arithmetic and copies ran while one was open for 7% -> 7% of each run, Pallas kernels for 0% -> 0%
where the time goes in v1:
time: 533 us; the launch traced here: 532 us
  waiting for transfers between devices  300 us (56%)
  blocking collectives  163 us (31%)
  matrix products  29.3 us (5%)
  between operations  16.4 us (3%)
  local copies, waits for them, and re-layouts  13.5 us (3%)
  other arithmetic  5.91 us (1%)
    reduce_scatter x1, waiting for transfers between devices, local(): lax.psum_scatter(low_point, 'fs', scatter_dimension=0, tiled=True)  61.8 us
    reduce_scatter x1, waiting for transfers between devices, local(): lax.psum_scatter(low_gate, 'fs', scatter_dimension=0, tiled=True)  52.9 us
    all_gather x1, waiting for transfers between devices, local(): lax.all_gather(new_g.astype(jnp.bfloat16), 'fs', axis=0, tiled=True)  46.5 us
    all_gather x1, waiting for transfers between devices, local(): lax.all_gather(factor_gate, 'fs', axis=0, tiled=True)  40 us
    all_gather x1, waiting for transfers between devices, local(): lax.all_gather(factor_value, 'fs', axis=0, tiled=True)  39.3 us
    psum x1, blocking collectives, local(): lax.psum((jnp.sum(full_v * full_v), jnp.sum(full_g * full_g), jnp.sum(ful...  37.8 us
    all_gather x1, blocking collectives, local(): lax.all_gather(factor_point, 'fs', axis=0, tiled=True)  33.4 us
    reduce_scatter x1, waiting for transfers between devices, local(): lax.psum_scatter(low_value, 'fs', scatter_dimension=0, tiled=True)  32.7 us
  transfers between devices with their start and end apart: 10, of which 9 were waited for; matrix products, arithmetic and copies ran while one was open for 7% of the time, Pallas kernels for 0%

profile of v1, /device:TPU:0, one launch (start us, length us, event | category | flops | bytes accessed | tf_op | source)
XLA Modules:
  0.0 532.1 jit_solution(13376494202518888004)
XLA Ops:
  7.2 0.0 copy-start
  7.2 0.0 reduce-scatter.8.cloned.1.call-start
  7.2 33.4 %all_gather.28 = bf16[1024,256]{1,0:T(8,128)(2,1)S(1)} all-gather(bf16[128,256]{1,0:T(8,128)(2,1)} %param.27), channel_id=1, replica_groups=mesh['fs'=8,'tp'=4] {'fs'}, dimensions={0}, use_global_device_ids=true | all-gather | bytes 589824 | tf_op jit(solution)/shard_map/all_gather | solution.py:73
  40.6 3.5 fusion.22
  44.1 0.5 fusion.1
  44.6 0.0 copy-start.8
  44.6 0.0 copy-start.9
  44.6 0.0 copy-start.5
  44.6 1.2 convolution_add_fusion
  45.8 0.0 reduce-scatter.8.cloned.1.call-update
  45.8 0.0 all-gather.7.cloned.1.call-start
  45.9 0.7 all-gather.7.cloned.1.call-update
  46.6 0.0 all-gather.5.cloned.1.call-start
  46.6 0.7 all-gather.5.cloned.1.call-update
  47.3 0.0 reduce-scatter.6.cloned.1.call-start
  47.4 61.8 %reduce-scatter.8.cloned.1.call-done = f32[32,256]{1,0:T(8,128)} async-done(((f32[256,256]{1,0:T(8,128)}), f32[32,256]{1,0:T(8,128)}) %reduce-scatter.8.cloned.1.call-update) | async-done | bytes 32784 | tf_op jit(solution)/shard_map/reduce_scatter | solution.py:82
  109.2 1.4 add_divide_fusion
  110.6 1.4 collective-permute-start
  112.0 2.5 collective-permute-done
  114.5 1.5 collective-permute-start.1
  116.0 0.2 copy.29
  116.2 4.0 collective-permute-done.1
  120.3 0.0 copy-start.1
  120.3 0.7 collective-permute-start.2
  121.0 40.0 %all-gather.7.cloned.1.call-done = bf16[4096,256]{1,0:T(8,128)(2,1)} async-done(((bf16[512,256]{1,0:T(8,128)(2,1)}), bf16[4096,256]{1,0:T(8,128)(2,1)}) %all-gather.7.cloned.1.call-update) | async-done | bytes 2097168 | tf_op jit(solution)/shard_map/all_gather | solution.py:67
  161.0 8.7 %fusion.21 = f32[2048,256]{1,0:T(8,128)S(1)} fusion(bf16[2048,4096]{1,0:T(8,128)(2,1)} %param.17, bf16[4096,256]{1,0:T(8,128)(2,1)} %all-gather.7.cloned.1.call-done), kind=kOutput, calls=%fused_computation.45 | convolution fusion | flops 4294967296 | bytes 20971520 | tf_op jit(solution)/shard_map/dot_general | solution.py:65
  169.7 0.5 fusion.4
  170.2 1.2 convolution_add_fusion.1
  171.4 0.0 reduce-scatter.6.cloned.1.call-update
  171.4 0.0 reduce-scatter.4.cloned.1.call-start
  171.5 39.3 %all-gather.5.cloned.1.call-done = bf16[4096,256]{1,0:T(8,128)(2,1)} async-done(((bf16[512,256]{1,0:T(8,128)(2,1)}), bf16[4096,256]{1,0:T(8,128)(2,1)}) %all-gather.5.cloned.1.call-update) | async-done | bytes 2097168 | tf_op jit(solution)/shard_map/all_gather | solution.py:62
  210.8 8.7 %fusion.20 = f32[2048,256]{1,0:T(8,128)S(1)} fusion(bf16[2048,4096]{1,0:T(8,128)(2,1)} %param.17, bf16[4096,256]{1,0:T(8,128)(2,1)} %all-gather.5.cloned.1.call-done), kind=kOutput, calls=%fused_computation.44 | convolution fusion | flops 4294967296 | bytes 20971520 | tf_op jit(solution)/shard_map/dot_general | solution.py:60
  219.5 0.5 fusion.7
  220.0 0.0 copy-start.11
  220.0 0.0 copy-start.3
  220.0 1.2 convolution_add_fusion.2
  221.2 0.0 reduce-scatter.4.cloned.1.call-update
  221.3 0.0 all-gather.9.cloned.1.call-start
  221.3 1.0 multiply_reduce_fusion.2
  222.3 52.9 %reduce-scatter.6.cloned.1.call-done = f32[32,256]{1,0:T(8,128)} async-done(((f32[256,256]{1,0:T(8,128)}), f32[32,256]{1,0:T(8,128)}) %reduce-scatter.6.cloned.1.call-update) | async-done | bytes 32784 | tf_op jit(solution)/shard_map/reduce_scatter | solution.py:81
  275.2 1.4 add_divide_fusion.1
  276.6 30.9 %all_gather.27 = f32[256,256]{1,0:T(8,128)S(1)} all-gather(f32[32,256]{1,0:T(8,128)S(1)} %get-tuple-element.36), channel_id=1, replica_groups=mesh['fs'=8,'tp'=4] {'fs'}, dimensions={0}, use_global_device_ids=true | all-gather | bytes 294912 | tf_op jit(solution)/shard_map/all_gather | solution.py:89
  307.5 32.7 %reduce-scatter.4.cloned.1.call-done = f32[32,256]{1,0:T(8,128)} async-done(((f32[256,256]{1,0:T(8,128)}), f32[32,256]{1,0:T(8,128)}) %reduce-scatter.4.cloned.1.call-update) | async-done | bytes 32784 | tf_op jit(solution)/shard_map/reduce_scatter | solution.py:80
  340.2 1.4 add_divide_fusion.2
  341.6 30.9 %all_gather.25 = f32[256,256]{1,0:T(8,128)S(1)} all-gather(f32[32,256]{1,0:T(8,128)S(1)} %get-tuple-element.39), channel_id=1, replica_groups=mesh['fs'=8,'tp'=4] {'fs'}, dimensions={0}, use_global_device_ids=true | all-gather | bytes 294912 | tf_op jit(solution)/shard_map/all_gather | solution.py:88
  372.5 1.2 multiply_reduce_fusion.1
  373.7 1.2 multiply_reduce_fusion
  374.9 37.8 %all-reduce = (f32[]{:T(128)}, f32[]{:T(128)}, f32[]{:T(128)}) all-reduce(f32[]{:T(128)} %get-tuple-element.42, f32[]{:T(128)} %get-tuple-element.44, f32[]{:T(128)} %get-tuple-element.46), channel_id=1, replica_groups=mesh['fs'=8,'tp'=4] {'fs','tp'}, use_global_device_ids=true, to_apply=%region_2.0 | all-reduce | flops 3 | bytes 24 | tf_op jit(solution)/shard_map/psum | solution.py:95
  413.4 0.8 fusion.19
  414.3 0.0 all-gather.9.cloned.1.call-update
  414.3 0.0 all-gather.11.cloned.1.call-start
  414.3 1.2 copy.30
  416.3 0.8 fusion.18
  417.1 0.0 all-gather.11.cloned.1.call-update
  417.1 0.1 copy.31
  418.0 0.8 copy.34
  418.7 29.6 %all_gather.31 = bf16[1024,256]{0,1:T(8,128)(2,1)S(1)} all-gather(bf16[128,256]{0,1:T(8,128)(2,1)S(1)} %get-tuple-element.27), channel_id=1, replica_groups=mesh['fs'=8,'tp'=4] {'fs'}, dimensions={0}, use_global_device_ids=true | all-gather | bytes 589824 | tf_op jit(solution)/shard_map/all_gather | solution.py:107
  448.3 1.0 copy.37
  449.3 1.0 copy.32
  450.3 1.0 copy.33
  451.3 19.3 %all-gather.9.cloned.1.call-done = bf16[4096,256]{0,1:T(8,128)(2,1)} async-done(((bf16[512,256]{0,1:T(8,128)(2,1)}), bf16[4096,256]{0,1:T(8,128)(2,1)}) %all-gather.9.cloned.1.call-update) | async-done | bytes 2097168 | tf_op jit(solution)/shard_map/all_gather | solution.py:105
  470.6 4.1 copy.35
  474.7 46.5 %all-gather.11.cloned.1.call-done = bf16[4096,256]{0,1:T(8,128)(2,1)} async-done(((bf16[512,256]{0,1:T(8,128)(2,1)}), bf16[4096,256]{0,1:T(8,128)(2,1)}) %all-gather.11.cloned.1.call-update) | async-done | bytes 2097168 | tf_op jit(solution)/shard_map/all_gather | solution.py:106
  521.2 4.1 copy.36
  (21 shorter events, 0.1 us)
Async XLA Ops:
  7.2 36.9 %copy-start = (bf16[2048,256]{1,0:T(8,128)(2,1)S(1)}, bf16[2048,256]{1,0:T(8,128)(2,1)}, u32[]{:S(2)}) copy-start(bf16[2048,256]{1,0:T(8,128)(2,1)} %param.21) | copy-start | bytes 3145732
  7.2 102.0 %reduce-scatter.8.cloned.1.call-start = ((), (), s32[]{:S(2)}) async-start(), calls=%async_computation.7 | async-start | bytes 294912 | tf_op jit(solution)/shard_map/reduce_scatter | solution.py:82
  44.6 64.6 %copy-start.8 = (f32[32,256]{1,0:T(8,128)S(1)}, f32[32,256]{1,0:T(8,128)}, u32[]{:S(2)}) copy-start(f32[32,256]{1,0:T(8,128)} %param.33) | copy-start | bytes 98308
  44.6 64.6 %copy-start.9 = (f32[32,256]{1,0:T(8,128)S(1)}, f32[32,256]{1,0:T(8,128)}, u32[]{:S(2)}) copy-start(f32[32,256]{1,0:T(8,128)} %param.30) | copy-start | bytes 98308
  44.6 71.4 %copy-start.5 = (f32[512,256]{1,0:T(8,128)S(1)}, f32[512,256]{1,0:T(8,128)}, u32[]{:S(2)}) copy-start(f32[512,256]{1,0:T(8,128)} %param.22) | copy-start | bytes 1572868
  45.8 115.1 %all-gather.7.cloned.1.call-start = ((), (), s32[]{:S(2)}) async-start(), calls=%async_computation.5 | async-start | bytes 2359296 | tf_op jit(solution)/shard_map/all_gather | solution.py:67
  46.6 164.1 %all-gather.5.cloned.1.call-start = ((), (), s32[]{:S(2)}) async-start(), calls=%async_computation.3 | async-start | bytes 2359296 | tf_op jit(solution)/shard_map/all_gather | solution.py:62
  47.3 227.8 %reduce-scatter.6.cloned.1.call-start = ((), (), s32[]{:S(2)}) async-start(), calls=%async_computation.6 | async-start | bytes 294912 | tf_op jit(solution)/shard_map/reduce_scatter | solution.py:81
  110.6 3.9 collective-permute-start
  114.5 5.7 %collective-permute-start.1 = (f32[64,256]{1,0:T(8,128)S(1)}, f32[64,256]{1,0:T(8,128)S(1)}, u32[]{:S(2)}, u32[]{:S(2)}) collective-permute-start(f32[64,256]{1,0:T(8,128)S(1)} %maximum_select_fusion.3), channel_id=1, source_target_pairs={{0,8},{4,12},{8,0},{12,4},{16,24},{20,28},{24,16},{28,20},{1,9},{5... | collective-permute-start | bytes 196616 | tf_op jit(solution)/shard_map/ppermute | solution.py:49
  120.3 49.4 %copy-start.1 = (bf16[2048,256]{1,0:T(8,128)(2,1)S(1)}, bf16[2048,256]{1,0:T(8,128)(2,1)}, u32[]{:S(2)}) copy-start(bf16[2048,256]{1,0:T(8,128)(2,1)} %param.19) | copy-start | bytes 3145732
  120.3 101.0 %collective-permute-start.2 = (f32[128,256]{1,0:T(8,128)S(1)}, f32[128,256]{1,0:T(8,128)S(1)}, u32[]{:S(2)}, u32[]{:S(2)}) collective-permute-start(f32[128,256]{1,0:T(8,128)S(1)} %maximum_select_fusion.2), channel_id=1, source_target_pairs={{0,16},{4,20},{8,24},{12,28},{16,0},{20,4},{24,8},{28,12},{1,17},{... | collective-permute-start | bytes 393224 | tf_op jit(solution)/shard_map/ppermute | solution.py:49
  171.4 48.1 %copy-start.2 = (bf16[2048,256]{1,0:T(8,128)(2,1)S(1)}, bf16[2048,256]{1,0:T(8,128)(2,1)}, u32[]{:S(2)}) copy-start(bf16[2048,256]{1,0:T(8,128)(2,1)} %param.18) | copy-start | bytes 3145732
  171.4 168.7 %reduce-scatter.4.cloned.1.call-start = ((), (), s32[]{:S(2)}) async-start(), calls=%async_computation.4 | async-start | bytes 294912 | tf_op jit(solution)/shard_map/reduce_scatter | solution.py:80
  220.0 1.3 copy-start.7
  220.0 55.2 %copy-start.10 = (f32[32,256]{1,0:T(8,128)S(1)}, f32[32,256]{1,0:T(8,128)}, u32[]{:S(2)}) copy-start(f32[32,256]{1,0:T(8,128)} %param.32) | copy-start | bytes 98308
  220.0 55.2 %copy-start.11 = (f32[32,256]{1,0:T(8,128)S(1)}, f32[32,256]{1,0:T(8,128)}, u32[]{:S(2)}) copy-start(f32[32,256]{1,0:T(8,128)} %param.29) | copy-start | bytes 98308
  220.0 152.5 %copy-start.3 = (bf16[512,256]{1,0:T(8,128)(2,1)S(1)}, bf16[512,256]{1,0:T(8,128)(2,1)}, u32[]{:S(2)}) copy-start(bf16[512,256]{1,0:T(8,128)(2,1)} %param.25) | copy-start | bytes 786436
  221.2 152.5 %copy-start.4 = (bf16[512,256]{1,0:T(8,128)(2,1)S(1)}, bf16[512,256]{1,0:T(8,128)(2,1)}, u32[]{:S(2)}) copy-start(bf16[512,256]{1,0:T(8,128)(2,1)} %param.26) | copy-start | bytes 786436
  221.3 249.3 %all-gather.9.cloned.1.call-start = ((), (), s32[]{:S(2)}) async-start(), calls=%async_computation.8 | async-start | bytes 2359296 | tf_op jit(solution)/shard_map/all_gather | solution.py:105
  414.3 2.9 copy-start.6
  414.3 106.9 %all-gather.11.cloned.1.call-start = ((), (), s32[]{:S(2)}) async-start(), calls=%async_computation.9 | async-start | bytes 2359296 | tf_op jit(solution)/shard_map/all_gather | solution.py:106
Sparse Core Ops, SparseCore 0:
  46.0 63.1 reduce-scatter.7
  111.3 49.6 all-gather.6
  163.1 47.6 all-gather.4
  214.5 60.6 reduce-scatter.5
  278.9 61.2 reduce-scatter.3
  414.4 56.1 all-gather.8
  472.6 48.5 all-gather.10
